TPU v7x, 32 devices: a whole 2x2x4 slice. The times are simulated.
32 devices in a mesh: grp: 2 (over y), ep: 8 (over z, x), tp: 2 (over core).
Axes of the slice: x: 2, y: 2, z: 4, core: 2. Of those that a mesh axis runs over, the one named last changes fastest.
Arguments:
- tokens: bfloat16 [2048, 2048], P(('grp', 'ep')), parts along dimension 0, may hold values from -6 to 6
- in_gain: float32 [2048], replicated, may hold values from 0.1 to 1.9
- routing: int32 [2048, 4], P(('grp', 'ep')), parts along dimension 0, may hold values from 0 to 15, as said below
- gate_prob: float32 [2048, 4], P(('grp', 'ep')), parts along dimension 0, may hold values from 0.05 to 1
- w_gate: bfloat16 [16, 2048, 512], P('ep', None, 'tp'), may hold values from -0.125 to 0.125
- w_up: bfloat16 [16, 2048, 512], P('ep', None, 'tp'), may hold values from -0.125 to 0.125
- w_down: bfloat16 [16, 512, 2048], P('ep', 'tp')
- out_gain: float32 [2048], P('tp'), may hold values from 0.1 to 1.9
Outputs:
- output: bfloat16 [2048, 2048], P(('grp', 'ep'), 'tp'), parts along dimension 0
There are 2 independent parts, one for each index of `grp`. A program takes and returns all parts, laid end to end along the dimension named above; an argument that names none is the same for every part. Nothing has to cross between parts.
Inputs may be any that keep to these rules, and one draw needn't show every extreme that they name: `routing`: each row names 4 different experts, all of one group (the same value of expert // 4). In the rows of one device no expert is named more than 64 times, and in every device's rows some expert is named exactly 64 times.
All inputs are finite; a program needn't handle non-finite values.
Results may differ from a plain program's by a relative error of at most 0.0077.
Values may be sent and summed in bfloat16 or wider, within the bound.
A program may use at most 64 MiB of HBM per device.

v0:
```python
import jax
import jax.numpy as jnp
from jax import lax
from jax.sharding import PartitionSpec as P

GROUPS = 4
EPS = 1e-06


def slot_ranks(flat_routes, expert_count):
    matches = (flat_routes[:, None] == jnp.arange(expert_count, dtype=jnp.int32)[None, :]).astype(
        jnp.int32
    )
    earlier = jnp.cumsum(matches, axis=0) - matches
    return jnp.sum(earlier * matches, axis=1)


def fill_rows(source, entries):
    filled = entries > 0
    return jnp.where(
        filled[:, None], source[jnp.maximum(entries - 1, 0)], jnp.zeros((), source.dtype)
    )


def body(tokens, in_gain, routing, gate_prob, w_gate, w_up, w_down, out_gain):
    ep_count = lax.axis_size("ep")
    local_experts = w_gate.shape[0]
    expert_count = local_experts * ep_count
    tok_dev, top_count = routing.shape
    model_width = tokens.shape[1]
    half_width = out_gain.shape[0]
    group_width = expert_count // GROUPS
    row_cap = max(2, tok_dev * top_count // (2 * group_width))
    floats = tokens.astype(jnp.float32)
    normed = (
        floats * lax.rsqrt(jnp.mean(floats * floats, axis=-1, keepdims=True) + EPS) * in_gain
    ).astype(jnp.bfloat16)
    flat_routes = routing.reshape(-1)
    slot_rank = slot_ranks(flat_routes, expert_count)
    slot_ids = flat_routes * row_cap + slot_rank
    token_ids = jnp.arange(tok_dev * top_count, dtype=jnp.int32) // top_count
    slot_table = jnp.zeros((expert_count * row_cap,), jnp.int32).at[slot_ids].set(token_ids + 1)
    own_columns = lax.dynamic_slice_in_dim(normed, lax.axis_index("tp") * half_width, half_width, 1)
    sendbuf = fill_rows(own_columns, slot_table).reshape(
        ep_count, local_experts, row_cap, half_width
    )
    arrived = lax.all_to_all(sendbuf, "ep", split_axis=0, concat_axis=0, tiled=True)
    arrived = lax.all_gather(arrived, "tp", axis=3, tiled=True)
    gate_act = jnp.einsum("secd,edf->secf", arrived, w_gate, preferred_element_type=jnp.float32)
    up_act = jnp.einsum("secd,edf->secf", arrived, w_up, preferred_element_type=jnp.float32)
    hidden = (jax.nn.silu(gate_act) * up_act).astype(jnp.bfloat16)
    partial_out = jnp.einsum("secf,efd->secd", hidden, w_down, preferred_element_type=jnp.float32)
    results = lax.psum_scatter(
        partial_out.astype(jnp.bfloat16), "tp", scatter_dimension=3, tiled=True
    )
    returned = lax.all_to_all(results, "ep", split_axis=0, concat_axis=0, tiled=True).reshape(
        expert_count * row_cap, half_width
    )
    picked = returned[slot_ids].astype(jnp.float32).reshape(tok_dev, top_count, half_width)
    mixed_rows = jnp.sum(picked * gate_prob[:, :, None], axis=1)
    squares = jnp.sum(mixed_rows * mixed_rows, axis=1)
    total_squares = lax.psum(squares, "tp")
    inv_rms = lax.rsqrt(total_squares / model_width + EPS)
    return (mixed_rows * inv_rms[:, None] * out_gain).astype(jnp.bfloat16)


def solution(mesh):
    placed = (
        P(("grp", "ep"), None),
        P(),
        P(("grp", "ep"), None),
        P(("grp", "ep"), None),
        P("ep", None, "tp"),
        P("ep", None, "tp"),
        P("ep", "tp", None),
        P("tp"),
    )
    return jax.shard_map(
        body, mesh=mesh, in_specs=placed, out_specs=P(("grp", "ep"), "tp"), check_vma=False
    )
```

profile of v0, /device:TPU:0, one launch (start us, length us, event | category | flops | bytes accessed | tf_op | source)
XLA Modules:
  0.0 192.8 jit_solution(13421549271625434358)
XLA Ops:
  6.5 0.0 copy-start
  6.5 0.0 copy-start.1
  6.5 0.0 copy-start.4
  6.5 0.0 all-gather.2.cloned.1.call-start
  6.6 1.3 convert_element_type.34
  7.8 1.2 multiply_reduce_fusion.1
  9.1 0.0 copy-done.1
  9.1 0.1 copy.19
  9.2 0.1 eq.29
  9.3 0.1 eq.25
  9.4 1.2 reduce-window.6
  10.6 0.2 slice_reduce_fusion
  10.9 0.1 copy.18
  11.0 0.1 mul.77
  11.1 0.1 fusion.24
  11.2 2.4 %scatter_custom_fusion = s32[1024]{0:T(1024)S(1)} fusion(s32[512]{0:T(512)S(1)} %bitcast.63, s32[512]{0:T(512)S(1)} %fusion.26, s32[]{:T(128)} %constant.19.clone.1), kind=kCustom, calls=%fused_computation.42 | custom fusion | bytes 4100 | tf_op jit(solution)/shard_map/scatter | solution.py:42
  13.7 0.1 broadcast_in_dim.16
  13.8 0.0 copy-done.4
  13.8 0.1 fusion.20
  13.9 5.4 %gather_fusion = bf16[1024,1024]{1,0:T(8,128)(2,1)} fusion(bf16[128,1024]{1,0:T(8,128)(2,1)S(1)} %fusion.20, s32[1024]{0:T(1024)S(1)} %maximum_clamp_fusion), kind=kCustom, calls=%fused_computation | custom fusion | bytes 4198400 | tf_op jit(solution)/shard_map/gather | solution.py:21
  19.3 1.8 broadcast_select_fusion
  21.1 55.3 %all_to_all.10 = bf16[8,2,64,1024]{3,2,1,0:T(8,128)(2,1)S(1)} all-to-all(bf16[8,2,64,1024]{3,2,1,0:T(8,128)(2,1)S(1)} %broadcast_select_fusion), channel_id=1, replica_groups=mesh['grp'=2,'ep'=8,'tp'=2] {'ep'}, dimensions={0} | all-to-all | bytes 4194304 | tf_op jit(solution)/shard_map/all_to_all | solution.py:47
  76.4 1.5 copy.22
  77.9 0.0 all-gather.2.cloned.1.call-update
  78.0 0.0 reduce-scatter.2.cloned.1.call-start
  78.0 12.8 %all-gather.2.cloned.1.call-done = bf16[8,2,64,2048]{3,2,0,1:T(8,128)(2,1)} async-done(((bf16[8,2,64,1024]{3,2,0,1:T(8,128)(2,1)}), bf16[8,2,64,2048]{3,2,0,1:T(8,128)(2,1)}) %all-gather.2.cloned.1.call-update) | async-done | bytes 4194320 | tf_op jit(solution)/shard_map/all_gather | solution.py:48
  90.8 4.1 %fusion.5 = f32[8,2,64,256]{3,2,0,1:T(8,128)S(1)} fusion(bf16[8,2,64,2048]{3,2,0,1:T(8,128)(2,1)} %all-gather.2.cloned.1.call-done, bf16[2,2048,256]{2,1,0:T(8,128)(2,1)} %param.12), kind=kOutput, calls=%fused_computation.11 | convolution fusion | flops 1073741824 | bytes 7340032 | tf_op jit(solution)/shard_map/secd,edf->secf/dot_general | solution.py:49
  94.9 0.0 copy-done
  94.9 7.3 %convert_bitcast_fusion = bf16[8,2,64,2048]{3,2,0,1:T(8,128)(2,1)} fusion(bf16[2,256,2048]{2,1,0:T(8,128)(2,1)S(1)} %copy-done, bf16[8,2,64,2048]{3,2,0,1:T(8,128)(2,1)} %all-gather.2.cloned.1.call-done, bf16[2,2048,256]{2,1,0:T(8,128)(2,1)} %param.13, f32[8,2,64,256]{3,2,0,1:T(8,128)S(1)} %fusion.5), kind=kOutput, calls=%fused_computation.3 | convolution fusion | flops 2151153664 | bytes 13631488 | tf_op jit(solution)/shard_map/secf,efd->secd/dot_general | solution.py:52
  102.2 0.0 reduce-scatter.2.cloned.1.call-update
  102.3 13.2 %reduce-scatter.2.cloned.1.call-done = bf16[8,2,64,1024]{3,2,0,1:T(8,128)(2,1)} async-done(((bf16[8,2,64,2048]{3,2,0,1:T(8,128)(2,1)}), bf16[8,2,64,1024]{3,2,0,1:T(8,128)(2,1)}) %reduce-scatter.2.cloned.1.call-update) | async-done | bytes 2097168 | tf_op jit(solution)/shard_map/reduce_scatter | solution.py:53
  115.5 3.1 %copy.23 = bf16[8,2,64,1024]{3,2,1,0:T(8,128)(2,1)} copy(bf16[8,2,64,1024]{3,2,0,1:T(8,128)(2,1)} %reduce-scatter.2.cloned.1.call-done) | data formatting | bytes 4194304 | tf_op jit(solution)/shard_map/reduce_scatter | solution.py:53
  118.6 0.0 copy-start.3
  118.6 6.0 %all-to-all-start.1 = ((bf16[8,2,64,1024]{3,2,1,0:T(8,128)(2,1)}), bf16[8,2,64,1024]{3,2,1,0:T(8,128)(2,1)}, u32[]{:S(2)}, u32[]{:S(2)}) async-start(bf16[8,2,64,1024]{3,2,1,0:T(8,128)(2,1)} %copy.23), calls=%async_computation.2 | async-start | bytes 4194304 | tf_op jit(solution)/shard_map/all_to_all | solution.py:56
  124.6 0.0 copy-done.3
  124.6 0.1 copy.24
  124.7 48.5 %all-to-all-done.1 = bf16[8,2,64,1024]{3,2,1,0:T(8,128)(2,1)} async-done(((bf16[8,2,64,1024]{3,2,1,0:T(8,128)(2,1)}), bf16[8,2,64,1024]{3,2,1,0:T(8,128)(2,1)}, u32[]{:S(2)}, u32[]{:S(2)}) %all-to-all-start.1) | async-done | bytes 2097184 | tf_op jit(solution)/shard_map/all_to_all | solution.py:56
  173.3 4.6 %gather_fusion.1 = bf16[512,1024]{1,0:T(8,128)(2,1)S(1)} fusion(bf16[1024,1024]{1,0:T(8,128)(2,1)} %bitcast.13, s32[1024]{0:T(1024)S(1)} %pad_clamp_fusion), kind=kCustom, calls=%fused_computation.1 | custom fusion | bytes 2099200 | tf_op jit(solution)/shard_map/gather | solution.py:59
  177.9 1.7 reshape.75
  179.6 0.0 copy-start.2
  179.6 3.0 %multiply_reduce_fusion = f32[128,1024]{1,0:T(8,128)S(1)} fusion(f32[128,4,1024]{2,1,0:T(4,128)} %reshape.75, f32[128,4]{1,0:T(8,128)S(1)} %copy.24), kind=kLoop, calls=%fused_computation.9 | loop fusion | flops 917504 | bytes 2623488 | tf_op jit(solution)/shard_map/reduce_sum | solution.py:60
  182.6 0.1 multiply_reduce_fusion.2
  182.7 2.5 %psum.7 = f32[128]{0:T(128)S(1)} all-reduce(f32[128]{0:T(128)S(1)} %multiply_reduce_fusion.2), channel_id=1, replica_groups=mesh['grp'=2,'ep'=8,'tp'=2] {'tp'}, use_global_device_ids=true, to_apply=%region_8.9 | all-reduce | flops 128 | bytes 1024 | tf_op jit(solution)/shard_map/psum | solution.py:62
  185.2 0.0 copy-done.2
  185.2 0.8 multiply_convert_fusion
  (12 shorter events, 0.1 us)
Async XLA Ops:
  6.5 88.4 %copy-start = (bf16[2,256,2048]{2,1,0:T(8,128)(2,1)S(1)}, bf16[2,256,2048]{2,1,0:T(8,128)(2,1)}, u32[]{:S(2)}) copy-start(bf16[2,256,2048]{2,1,0:T(8,128)(2,1)} %param.14) | copy-start | bytes 6291460
  6.5 2.5 %copy-start.1 = (s32[128,4]{0,1:T(4,128)S(1)}, s32[128,4]{0,1:T(4,128)}, u32[]{:S(2)}) copy-start(s32[128,4]{0,1:T(4,128)} %param.10) | copy-start | bytes 6148
  6.5 7.2 %copy-start.4 = (f32[2048]{0:T(1024)S(1)}, f32[2048]{0:T(1024)}, u32[]{:S(2)}) copy-start(f32[2048]{0:T(1024)} %param.9) | copy-start | bytes 24580
  6.5 84.3 %all-gather.2.cloned.1.call-start = ((), (), s32[]{:S(2)}) async-start(), calls=%async_computation.3 | async-start | bytes 6291456 | tf_op jit(solution)/shard_map/all_gather | solution.py:48
  78.0 37.5 %reduce-scatter.2.cloned.1.call-start = ((), (), s32[]{:S(2)}) async-start(), calls=%async_computation.4 | async-start | bytes 6291456 | tf_op jit(solution)/shard_map/reduce_scatter | solution.py:53
  118.6 6.0 %copy-start.3 = (f32[128,4]{0,1:T(4,128)S(1)}, f32[128,4]{0,1:T(4,128)}, u32[]{:S(2)}) copy-start(f32[128,4]{0,1:T(4,128)} %param.11) | copy-start | bytes 6148
  118.6 54.7 %all-to-all-start.1 = ((bf16[8,2,64,1024]{3,2,1,0:T(8,128)(2,1)}), bf16[8,2,64,1024]{3,2,1,0:T(8,128)(2,1)}, u32[]{:S(2)}, u32[]{:S(2)}) async-start(bf16[8,2,64,1024]{3,2,1,0:T(8,128)(2,1)} %copy.23), calls=%async_computation.2 | async-start | bytes 4194304 | tf_op jit(solution)/shard_map/all_to_all | solution.py:56
  179.6 5.6 %copy-start.2 = (f32[1024]{0:T(1024)S(1)}, f32[1024]{0:T(1024)}, u32[]{:S(2)}) copy-start(f32[1024]{0:T(1024)} %param.15) | copy-start | bytes 12292
Sparse Core Ops, SparseCore 0:
  78.1 12.6 all-gather.1
  102.4 13.0 reduce-scatter.1
where the time goes:
time: 193 us
  waiting for transfers between devices  74.6 us (39%)
  blocking collectives  57.8 us (30%)
  local copies, waits for them, and re-layouts  19.8 us (10%)
  between operations  13.6 us (7%)
  matrix products  11.4 us (6%)
  other arithmetic  9.68 us (5%)
  starting transfers between devices  6.06 us (3%)
    all_to_all x1, blocking collectives, body(): lax.all_to_all(sendbuf, 'ep', split_axis=0, concat_axis=0, tiled=True)  55.3 us
    all_to_all x1, waiting for transfers between devices, body(): lax.all_to_all(results, 'ep', split_axis=0, concat_axis=0, tiled=True)  48.5 us
    reduce_scatter x1, waiting for transfers between devices, body(): lax.psum_scatter(partial_out.astype(jnp.bfloat16), 'tp', scatter_dimensio...  13.2 us
    all_gather x1, waiting for transfers between devices, body(): arrived = lax.all_gather(arrived, 'tp', axis=3, tiled=True)  12.8 us
    dot_general x1, matrix products, body(): jnp.einsum('secf,efd->secd', hidden, w_down, preferred_element_type=jnp.f...  7.3 us
    all_to_all x1, starting transfers between devices, body(): lax.all_to_all(results, 'ep', split_axis=0, concat_axis=0, tiled=True)  6.02 us
    gather x1, local copies, waits for them, and re-layouts, fill_rows(): source[jnp.maximum(entries - 1, 0)]  5.36 us
    gather x1, local copies, waits for them, and re-layouts, body(): returned[slot_ids].astype(jnp.float32)  4.59 us
  transfers between devices with their start and end apart: 3, of which 3 were waited for; matrix products, arithmetic and copies ran while one was open for 0% of the time, Pallas kernels for 0%

commit v1 on v0

--- a/solution.py
+++ b/solution.py
@@ -5,6 +5,9 @@
 
 GROUPS = 4
 EPS = 1e-06
+group_quarters = lambda load, mesh_name: jnp.concatenate(
+    lax.all_gather(load, axis_name=mesh_name), axis=3
+)
 
 
 def slot_ranks(flat_routes, expert_count):
@@ -45,7 +48,7 @@
         ep_count, local_experts, row_cap, half_width
     )
     arrived = lax.all_to_all(sendbuf, "ep", split_axis=0, concat_axis=0, tiled=True)
-    arrived = lax.all_gather(arrived, "tp", axis=3, tiled=True)
+    arrived = group_quarters(arrived, "tp")
     gate_act = jnp.einsum("secd,edf->secf", arrived, w_gate, preferred_element_type=jnp.float32)
     up_act = jnp.einsum("secd,edf->secf", arrived, w_up, preferred_element_type=jnp.float32)
     hidden = (jax.nn.silu(gate_act) * up_act).astype(jnp.bfloat16)

time: 193 us -> 208 us (1.078)
  local copies, waits for them, and re-layouts: 19.8 us -> 34.5 us
    reshape x0 -> x2, local copies, waits for them, and re-layouts: none -> 16.3 us  [jnp.concatenate(lax.all_gather(load, axis_name=mesh_name), axis=3)]
where the time goes in v1:
time: 208 us
  waiting for transfers between devices  74.6 us (36%)
  blocking collectives  57.9 us (28%)
  local copies, waits for them, and re-layouts  34.5 us (17%)
  between operations  13.6 us (7%)
  matrix products  11.4 us (5%)
  other arithmetic  9.68 us (5%)
  starting transfers between devices  6.07 us (3%)
    all_to_all x1, blocking collectives, body(): lax.all_to_all(sendbuf, 'ep', split_axis=0, concat_axis=0, tiled=True)  55.4 us
    all_to_all x1, waiting for transfers between devices, body(): lax.all_to_all(results, 'ep', split_axis=0, concat_axis=0, tiled=True)  48.5 us
    reshape x2, local copies, waits for them, and re-layouts, jnp.concatenate(lax.all_gather(load, axis_name=mesh_name), axis=3)  16.3 us
    reduce_scatter x1, waiting for transfers between devices, body(): lax.psum_scatter(partial_out.astype(jnp.bfloat16), 'tp', scatter_dimensio...  13.2 us
    all_gather x1, waiting for transfers between devices, lax.all_gather(load, axis_name=mesh_name)  12.8 us
    dot_general x1, matrix products, body(): jnp.einsum('secf,efd->secd', hidden, w_down, preferred_element_type=jnp.f...  7.3 us
    all_to_all x1, starting transfers between devices, body(): lax.all_to_all(results, 'ep', split_axis=0, concat_axis=0, tiled=True)  6.02 us
    gather x1, local copies, waits for them, and re-layouts, fill_rows(): source[jnp.maximum(entries - 1, 0)]  5.36 us
  transfers between devices with their start and end apart: 3, of which 3 were waited for; matrix products, arithmetic and copies ran while one was open for 0% of the time, Pallas kernels for 0%

profile of v1, /device:TPU:0, one launch (start us, length us, event | category | flops | bytes accessed | tf_op | source)
XLA Modules:
  0.0 207.7 jit_solution(15831142377028312146)
XLA Ops:
  6.5 0.0 copy-start
  6.5 0.0 copy-start.1
  6.5 0.0 copy-start.4
  6.5 0.0 all-gather.3.cloned.1.call-start
  6.6 1.3 convert_element_type.34
  7.8 1.2 multiply_reduce_fusion.1
  9.1 0.0 copy-done.1
  9.1 0.1 copy.18
  9.2 0.1 eq.29
  9.3 0.1 eq.25
  9.4 1.2 reduce-window.6
  10.6 0.2 slice_reduce_fusion
  10.9 0.1 copy.17
  11.0 0.1 mul.77
  11.1 0.1 fusion.24
  11.2 2.4 %scatter_custom_fusion = s32[1024]{0:T(1024)S(1)} fusion(s32[512]{0:T(512)S(1)} %bitcast.69, s32[512]{0:T(512)S(1)} %fusion.26, s32[]{:T(128)} %constant.19.clone.1), kind=kCustom, calls=%fused_computation.42 | custom fusion | bytes 4100 | tf_op jit(solution)/shard_map/scatter | solution.py:45
  13.7 0.1 broadcast_in_dim.16
  13.8 0.0 copy-done.4
  13.8 0.1 fusion.20
  13.9 5.4 %gather_fusion = bf16[1024,1024]{1,0:T(8,128)(2,1)} fusion(bf16[128,1024]{1,0:T(8,128)(2,1)S(1)} %fusion.20, s32[1024]{0:T(1024)S(1)} %maximum_clamp_fusion), kind=kCustom, calls=%fused_computation | custom fusion | bytes 4198400 | tf_op jit(solution)/shard_map/gather | solution.py:24
  19.3 1.8 broadcast_select_fusion
  21.1 55.4 %all_to_all.10 = bf16[8,2,64,1024]{3,2,1,0:T(8,128)(2,1)} all-to-all(bf16[8,2,64,1024]{3,2,1,0:T(8,128)(2,1)S(1)} %broadcast_select_fusion), channel_id=1, replica_groups=mesh['grp'=2,'ep'=8,'tp'=2] {'ep'}, dimensions={0} | all-to-all | bytes 4194304 | tf_op jit(solution)/shard_map/all_to_all | solution.py:50
  76.5 0.0 all-gather.3.cloned.1.call-update
  76.5 0.0 reduce-scatter.2.cloned.1.call-start
  76.6 12.8 %all-gather.3.cloned.1.call-done = bf16[16,2,64,1024]{3,2,1,0:T(8,128)(2,1)} async-done(((bf16[8,2,64,1024]{3,2,1,0:T(8,128)(2,1)}), bf16[16,2,64,1024]{3,2,1,0:T(8,128)(2,1)}) %all-gather.3.cloned.1.call-update) | async-done | bytes 4194320 | tf_op jit(solution)/shard_map/all_gather | solution.py:9
  89.4 8.5 %copy.21 = bf16[8,2,64,2,1024]{4,3,2,0,1:T(2,128)(2,1)} copy(bf16[8,2,64,2,1024]{4,2,1,0,3:T(8,128)(2,1)} %bitcast.68) | data formatting | bytes 8388608 | tf_op jit(solution)/shard_map/reshape | solution.py:8
  97.9 7.8 %reshape.81 = bf16[8,2,64,2048]{3,2,0,1:T(8,128)(2,1)} reshape(bf16[8,2,64,2,1024]{4,3,2,0,1:T(2,128)(2,1)} %copy.21) | data formatting | bytes 8388608 | tf_op jit(solution)/shard_map/reshape | solution.py:8
  105.6 4.1 %fusion.5 = f32[8,2,64,256]{3,2,0,1:T(8,128)S(1)} fusion(bf16[8,2,64,2048]{3,2,0,1:T(8,128)(2,1)} %reshape.81, bf16[2,2048,256]{2,1,0:T(8,128)(2,1)} %param.12), kind=kOutput, calls=%fused_computation.11 | convolution fusion | flops 1073741824 | bytes 7340032 | tf_op jit(solution)/shard_map/secd,edf->secf/dot_general | solution.py:52
  109.8 0.0 copy-done
  109.8 7.3 %convert_bitcast_fusion = bf16[8,2,64,2048]{3,2,0,1:T(8,128)(2,1)} fusion(bf16[2,256,2048]{2,1,0:T(8,128)(2,1)S(1)} %copy-done, bf16[8,2,64,2048]{3,2,0,1:T(8,128)(2,1)} %reshape.81, bf16[2,2048,256]{2,1,0:T(8,128)(2,1)} %param.13, f32[8,2,64,256]{3,2,0,1:T(8,128)S(1)} %fusion.5), kind=kOutput, calls=%fused_computation.3 | convolution fusion | flops 2151153664 | bytes 13631488 | tf_op jit(solution)/shard_map/secf,efd->secd/dot_general | solution.py:55
  117.1 0.0 reduce-scatter.2.cloned.1.call-update
  117.1 13.2 %reduce-scatter.2.cloned.1.call-done = bf16[8,2,64,1024]{3,2,0,1:T(8,128)(2,1)} async-done(((bf16[8,2,64,2048]{3,2,0,1:T(8,128)(2,1)}), bf16[8,2,64,1024]{3,2,0,1:T(8,128)(2,1)}) %reduce-scatter.2.cloned.1.call-update) | async-done | bytes 2097168 | tf_op jit(solution)/shard_map/reduce_scatter | solution.py:56
  130.3 3.1 %copy.22 = bf16[8,2,64,1024]{3,2,1,0:T(8,128)(2,1)} copy(bf16[8,2,64,1024]{3,2,0,1:T(8,128)(2,1)} %reduce-scatter.2.cloned.1.call-done) | data formatting | bytes 4194304 | tf_op jit(solution)/shard_map/reduce_scatter | solution.py:56
  133.4 0.0 copy-start.3
  133.4 6.0 %all-to-all-start.1 = ((bf16[8,2,64,1024]{3,2,1,0:T(8,128)(2,1)}), bf16[8,2,64,1024]{3,2,1,0:T(8,128)(2,1)}, u32[]{:S(2)}, u32[]{:S(2)}) async-start(bf16[8,2,64,1024]{3,2,1,0:T(8,128)(2,1)} %copy.22), calls=%async_computation.2 | async-start | bytes 4194304 | tf_op jit(solution)/shard_map/all_to_all | solution.py:59
  139.4 0.0 copy-done.3
  139.5 0.1 copy.23
  139.6 48.5 %all-to-all-done.1 = bf16[8,2,64,1024]{3,2,1,0:T(8,128)(2,1)} async-done(((bf16[8,2,64,1024]{3,2,1,0:T(8,128)(2,1)}), bf16[8,2,64,1024]{3,2,1,0:T(8,128)(2,1)}, u32[]{:S(2)}, u32[]{:S(2)}) %all-to-all-start.1) | async-done | bytes 2097184 | tf_op jit(solution)/shard_map/all_to_all | solution.py:59
  188.1 4.6 %gather_fusion.1 = bf16[512,1024]{1,0:T(8,128)(2,1)S(1)} fusion(bf16[1024,1024]{1,0:T(8,128)(2,1)} %bitcast.15, s32[1024]{0:T(1024)S(1)} %pad_clamp_fusion), kind=kCustom, calls=%fused_computation.1 | custom fusion | bytes 2099200 | tf_op jit(solution)/shard_map/gather | solution.py:62
  192.7 1.7 reshape.83
  194.4 0.0 copy-start.2
  194.4 3.0 %multiply_reduce_fusion = f32[128,1024]{1,0:T(8,128)S(1)} fusion(f32[128,4,1024]{2,1,0:T(4,128)} %reshape.83, f32[128,4]{1,0:T(8,128)S(1)} %copy.23), kind=kLoop, calls=%fused_computation.9 | loop fusion | flops 917504 | bytes 2623488 | tf_op jit(solution)/shard_map/reduce_sum | solution.py:63
  197.4 0.1 multiply_reduce_fusion.2
  197.5 2.5 %psum.7 = f32[128]{0:T(128)S(1)} all-reduce(f32[128]{0:T(128)S(1)} %multiply_reduce_fusion.2), channel_id=1, replica_groups=mesh['grp'=2,'ep'=8,'tp'=2] {'tp'}, use_global_device_ids=true, to_apply=%region_8.9 | all-reduce | flops 128 | bytes 1024 | tf_op jit(solution)/shard_map/psum | solution.py:65
  200.0 0.0 copy-done.2
  200.0 0.8 multiply_convert_fusion
  (12 shorter events, 0.1 us)
Async XLA Ops:
  6.5 103.2 %copy-start = (bf16[2,256,2048]{2,1,0:T(8,128)(2,1)S(1)}, bf16[2,256,2048]{2,1,0:T(8,128)(2,1)}, u32[]{:S(2)}) copy-start(bf16[2,256,2048]{2,1,0:T(8,128)(2,1)} %param.14) | copy-start | bytes 6291460
  6.5 2.5 %copy-start.1 = (s32[128,4]{0,1:T(4,128)S(1)}, s32[128,4]{0,1:T(4,128)}, u32[]{:S(2)}) copy-start(s32[128,4]{0,1:T(4,128)} %param.10) | copy-start | bytes 6148
  6.5 7.2 %copy-start.4 = (f32[2048]{0:T(1024)S(1)}, f32[2048]{0:T(1024)}, u32[]{:S(2)}) copy-start(f32[2048]{0:T(1024)} %param.9) | copy-start | bytes 24580
  6.5 82.8 %all-gather.3.cloned.1.call-start = ((), (), s32[]{:S(2)}) async-start(), calls=%async_computation.4 | async-start | bytes 6291456 | tf_op jit(solution)/shard_map/all_gather | solution.py:9
  76.5 53.8 %reduce-scatter.2.cloned.1.call-start = ((), (), s32[]{:S(2)}) async-start(), calls=%async_computation.3 | async-start | bytes 6291456 | tf_op jit(solution)/shard_map/reduce_scatter | solution.py:56
  133.4 6.0 %copy-start.3 = (f32[128,4]{0,1:T(4,128)S(1)}, f32[128,4]{0,1:T(4,128)}, u32[]{:S(2)}) copy-start(f32[128,4]{0,1:T(4,128)} %param.11) | copy-start | bytes 6148
  133.4 54.7 %all-to-all-start.1 = ((bf16[8,2,64,1024]{3,2,1,0:T(8,128)(2,1)}), bf16[8,2,64,1024]{3,2,1,0:T(8,128)(2,1)}, u32[]{:S(2)}, u32[]{:S(2)}) async-start(bf16[8,2,64,1024]{3,2,1,0:T(8,128)(2,1)} %copy.22), calls=%async_computation.2 | async-start | bytes 4194304 | tf_op jit(solution)/shard_map/all_to_all | solution.py:59
  194.4 5.6 %copy-start.2 = (f32[1024]{0:T(1024)S(1)}, f32[1024]{0:T(1024)}, u32[]{:S(2)}) copy-start(f32[1024]{0:T(1024)} %param.15) | copy-start | bytes 12292
Sparse Core Ops, SparseCore 0:
  76.6 12.6 all-gather.2
  117.2 13.0 reduce-scatter.1
